TPU v7x, 32 devices: a whole 2x2x4 slice. The times are simulated.
32 devices in a mesh: ep: 16 (over z, y, x), tp: 2 (over core).
Axes of the slice: x: 2, y: 2, z: 4, core: 2. Of those that a mesh axis runs over, the one named last changes fastest.
Arguments:
- hidden_in: bfloat16 [512, 2048], P('ep'), may hold values from -6 to 6
- past_lengths: int32 [512], P('ep'), may hold values from 1 to 1023, as said below
- key_cache: bfloat16 [512, 1024, 256], P('ep', None, 'tp'), may hold values from -512 to 512
- value_cache: bfloat16 [512, 1024, 256], P('ep', None, 'tp'), may hold values from -6 to 6
- attn_gain: float32 [2048], replicated, may hold values from 0.1 to 1.9
- w_query: bfloat16 [2048, 2048], P(None, 'tp'), may hold values from -0.125 to 0.125
- w_key: bfloat16 [2048, 256], P(None, 'tp'), may hold values from -0.125 to 0.125
- w_value: bfloat16 [2048, 256], P(None, 'tp'), may hold values from -0.125 to 0.125
- lambdas: float32 [16], P('tp'), may hold values from 0.3 to 0.8
- head_gain: float32 [128], replicated, may hold values from 0.1 to 1.9
- w_out: bfloat16 [2048, 2048], P('tp'), may hold values from -0.125 to 0.125
- ffn_gain: float32 [2048], replicated, may hold values from 0.1 to 1.9
- route_ids: int32 [512, 2], P('ep'), may hold values from 0 to 7, all different within a row; in each aligned block of 32 rows (0 to 31, 32 to 63, ...) at most 16 rows name the same one
- route_weights: float32 [512, 2], P('ep'), may hold values from 0.2 to 1
- expert_gate: bfloat16 [16, 2048, 704], P('ep', None, 'tp'), may hold values from -0.125 to 0.125
- expert_up: bfloat16 [16, 2048, 704], P('ep', None, 'tp'), may hold values from -0.125 to 0.125
- expert_down: bfloat16 [16, 704, 2048], P('ep', None, 'tp'), may hold values from -1.25 to 1.25
- gate_vector: bfloat16 [2048], replicated, may hold values from -0.125 to 0.125
- dense_gate: bfloat16 [2048, 5632], P(None, ('ep', 'tp')), may hold values from -0.125 to 0.125
- dense_up: bfloat16 [2048, 5632], P(None, ('ep', 'tp')), may hold values from -0.125 to 0.125
- dense_down: bfloat16 [5632, 2048], P('ep', 'tp'), may hold values from -0.625 to 0.625
Outputs:
- mixed_out: bfloat16 [512, 2048], P('ep', 'tp')
- new_keys: bfloat16 [512, 256], P('ep', 'tp')
- new_values: bfloat16 [512, 256], P('ep', 'tp')
Inputs may be any that keep to these rules, and one draw needn't show every extreme that they name: `past_lengths`: the new token of a sequence stands at this position; some sequence has 1023 cached positions in every draw. `route_ids`: each row names 2 different experts; among the rows of one index of ep no expert is named more than 16 times, a bound that some block reaches in every draw.
All inputs are finite; a program needn't handle non-finite values.
Results may differ from a plain program's by a relative error of at most 0.02.
The roundings to bfloat16 on the way count: a program that leaves them out, or rounds other values in their place, can miss the bound.
Values may be sent and summed in bfloat16 or wider, within the bound.
A program may use at most 128 MiB of HBM per device.

v0:
```python
import jax
import jax.numpy as jnp
from jax import lax
from jax.sharding import PartitionSpec as P

HEAD_DIM = 64
VALUE_DIM = 128
norm_eps = 1e-05
rope_base = 10000.0


def rms_rows(values, scales):
    values = values.astype(jnp.float32)
    return values * lax.rsqrt(jnp.mean(values * values, axis=-1, keepdims=True) + norm_eps) * scales


def rotary(values, position):
    middle = values.shape[-1] // 2
    inverse = rope_base ** (-jnp.arange(middle, dtype=jnp.float32) / middle)
    angles = position.astype(jnp.float32)[:, None] * inverse[None, :]
    cosine = jnp.cos(angles)[:, None, None, :]
    sine_part = jnp.sin(angles)[:, None, None, :]
    leading, second = (values[..., :middle], values[..., middle:])
    return jnp.concatenate(
        [leading * cosine - second * sine_part, second * cosine + leading * sine_part], axis=-1
    )


def per_device(
    hidden_in,
    past_lengths,
    key_cache,
    value_cache,
    attn_gain,
    w_query,
    w_key,
    w_value,
    lambdas,
    head_gain,
    w_out,
    ffn_gain,
    route_ids,
    route_weights,
    expert_gate,
    expert_up,
    expert_down,
    gate_vector,
    dense_gate,
    dense_up,
    dense_down,
):
    batch_rows = hidden_in.shape[0]
    model_width = hidden_in.shape[1]
    tp_count = lax.axis_size("tp")
    ep_count = lax.axis_size("ep")
    tp_rank = lax.axis_index("tp")
    half_width = model_width // tp_count
    heads_here = lambdas.shape[0]
    kv_here = w_key.shape[1] // (2 * HEAD_DIM)
    per_key = heads_here // kv_here
    scale_qk = HEAD_DIM ** (-0.5)
    normed = rms_rows(hidden_in, attn_gain).astype(jnp.bfloat16)
    queries = rotary(
        jnp.dot(normed, w_query, preferred_element_type=jnp.float32).reshape(
            batch_rows, heads_here, 2, HEAD_DIM
        ),
        past_lengths,
    ).astype(jnp.bfloat16)
    key_new = rotary(
        jnp.dot(normed, w_key, preferred_element_type=jnp.float32).reshape(
            batch_rows, kv_here, 2, HEAD_DIM
        ),
        past_lengths,
    ).astype(jnp.bfloat16)
    value_new = jnp.dot(normed, w_value, preferred_element_type=jnp.float32).astype(jnp.bfloat16)
    grouped = queries.reshape(batch_rows, kv_here, per_key, 2, HEAD_DIM)
    own_score = (
        jnp.einsum("sgamd,sgmd->sgam", grouped, key_new, preferred_element_type=jnp.float32)
        * scale_qk
    )
    value_rows = value_new.reshape(batch_rows, kv_here, 1, 1, VALUE_DIM).astype(jnp.float32)
    start_state = (
        own_score,
        jnp.ones_like(own_score),
        jnp.broadcast_to(value_rows, own_score.shape + (VALUE_DIM,)),
    )
    cache_len = key_cache.shape[1]
    span_len = min(256, cache_len)
    spans_needed = (jnp.max(past_lengths) + span_len - 1) // span_len

    def visit(block_index, carried):
        running, totals, summed = carried
        offset = block_index * span_len
        key_rows = lax.dynamic_slice_in_dim(key_cache, offset, span_len, 1).reshape(
            batch_rows, span_len, kv_here, 2, HEAD_DIM
        )
        cached = lax.dynamic_slice_in_dim(value_cache, offset, span_len, 1).reshape(
            batch_rows, span_len, kv_here, VALUE_DIM
        )
        scores = (
            jnp.einsum("sgamd,slgmd->sgaml", grouped, key_rows, preferred_element_type=jnp.float32)
            * scale_qk
        )
        usable = (offset + jnp.arange(span_len))[None, :] < past_lengths[:, None]
        scores = jnp.where(usable[:, None, None, None, :], scores, -jnp.inf)
        raised = jnp.maximum(running, jnp.max(scores, axis=-1))
        fading = jnp.exp(running - raised)
        weights = jnp.exp(scores - raised[..., None])
        totals = totals * fading + jnp.sum(weights, axis=-1)
        summed = summed * fading[..., None] + jnp.einsum(
            "sgaml,slge->sgame",
            weights.astype(jnp.bfloat16),
            cached,
            preferred_element_type=jnp.float32,
        )
        return (raised, totals, summed)

    running, totals, summed = lax.fori_loop(0, spans_needed, visit, start_state)
    mapped = summed / totals[..., None]
    head_mix = mapped[..., 0, :] - lambdas.reshape(1, kv_here, per_key, 1) * mapped[..., 1, :]
    head_out = rms_rows(head_mix, head_gain).astype(jnp.bfloat16).reshape(batch_rows, -1)
    attn_out = lax.psum(
        jnp.dot(head_out, w_out, preferred_element_type=jnp.float32).astype(jnp.bfloat16), "tp"
    )
    residual = hidden_in.astype(jnp.float32) + attn_out.astype(jnp.float32)
    moe_in = rms_rows(residual, ffn_gain).astype(jnp.bfloat16)
    mix_gate = jax.nn.sigmoid(
        jnp.dot(moe_in, gate_vector, preferred_element_type=jnp.float32)
    ).astype(jnp.bfloat16)
    top_count = route_ids.shape[1]
    experts = ep_count // 2
    capacity = max(2, 2 * batch_rows * top_count // experts)
    flat_ids = route_ids.reshape(-1)
    matches = (flat_ids[:, None] == jnp.arange(experts)[None, :]).astype(jnp.int32)
    earlier = jnp.sum((jnp.cumsum(matches, axis=0) - matches) * matches, axis=1)
    slot_of = flat_ids * capacity + earlier
    placing = (jnp.arange(experts * capacity)[:, None] == slot_of[None, :]).astype(jnp.float32)
    repeated = jnp.repeat(moe_in, top_count, axis=0)
    packed = jnp.dot(
        placing.astype(jnp.bfloat16), repeated, preferred_element_type=jnp.float32
    ).astype(jnp.bfloat16)
    outgoing = jnp.broadcast_to(
        packed.reshape(experts, 1, capacity, model_width), (experts, 2, capacity, model_width)
    ).reshape(ep_count, capacity, model_width)
    arrived = lax.all_to_all(outgoing, "ep", split_axis=0, concat_axis=0, tiled=True)
    leading = arrived.shape[:2]
    flat_rows = arrived.reshape(-1, model_width)
    gate_pre = jnp.dot(flat_rows, expert_gate[0], preferred_element_type=jnp.float32)
    up_pre = jnp.dot(flat_rows, expert_up[0], preferred_element_type=jnp.float32)
    inner_act = (jax.nn.silu(gate_pre) * up_pre).astype(jnp.bfloat16)
    inner_act = lax.all_gather(inner_act, "tp", axis=1, tiled=True)
    partial_value = jnp.dot(inner_act, expert_down[0], preferred_element_type=jnp.float32).reshape(
        leading + (half_width,)
    )
    returned = lax.all_to_all(
        partial_value.astype(jnp.bfloat16), "ep", split_axis=0, concat_axis=0, tiled=True
    ).astype(partial_value.dtype)
    paired = jnp.sum(returned.reshape(experts, 2, capacity, half_width), axis=1).reshape(
        experts * capacity, half_width
    )
    weighted = (
        (placing * route_weights.reshape(1, -1))
        .reshape(experts * capacity, batch_rows, top_count)
        .sum(axis=2)
    )
    moe_out = jnp.einsum("ct,cd->td", weighted, paired, precision=lax.Precision.HIGHEST)
    rows_all, gates_all = (
        lax.all_gather(moe_in, "ep", axis=0, tiled=True),
        lax.all_gather(mix_gate, "ep", axis=0, tiled=True),
    )
    local_pre = jnp.dot(rows_all, dense_gate, preferred_element_type=jnp.float32)
    local_up = jnp.dot(rows_all, dense_up, preferred_element_type=jnp.float32)
    local_act = (jax.nn.silu(local_pre) * local_up).astype(jnp.bfloat16)
    dense_act = lax.all_gather(local_act, "tp", axis=1, tiled=True)
    gate_rows = gates_all.astype(jnp.float32)
    dense_out = lax.psum_scatter(
        jnp.dot(dense_act, dense_down, preferred_element_type=jnp.float32) * gate_rows[:, None],
        "ep",
        scatter_dimension=0,
        tiled=True,
    )
    own_residual = lax.dynamic_slice_in_dim(residual, tp_rank * half_width, half_width, 1)
    mixed_out = (own_residual + moe_out + dense_out).astype(jnp.bfloat16)
    return (mixed_out, key_new.reshape(batch_rows, -1), value_new)


def solution(mesh):
    return jax.shard_map(
        per_device,
        mesh=mesh,
        in_specs=(
            P("ep", None),
            P("ep"),
            P("ep", None, "tp"),
            P("ep", None, "tp"),
            P(),
            P(None, "tp"),
            P(None, "tp"),
            P(None, "tp"),
            P("tp"),
            P(),
            P("tp", None),
            P(),
            P("ep", None),
            P("ep", None),
            P("ep", None, "tp"),
            P("ep", None, "tp"),
            P("ep", None, "tp"),
            P(),
            P(None, ("ep", "tp")),
            P(None, ("ep", "tp")),
            P("ep", "tp"),
        ),
        out_specs=(P("ep", "tp"), P("ep", "tp"), P("ep", "tp")),
        check_vma=False,
    )
```

profile of v0, /device:TPU:0, one launch (start us, length us, event | category | flops | bytes accessed | tf_op | source)
XLA Modules:
  0.0 262.9 jit_solution(17510185976092909314)
XLA Ops:
  7.2 1.4 fusion.67
  9.3 1.0 fusion.43
  10.4 1.4 fusion.62
  11.9 3.2 %fusion.60 = f32[32,1024]{1,0:T(8,128)S(1)} fusion(bf16[2048,1024]{1,0:T(8,128)(2,1)} %param.28, bf16[32,2048]{1,0:T(8,128)(2,1)} %param.23, f32[2048]{0:T(1024)} %param.27, f32[32]{0:T(128)S(1)} %add_rsqrt_fusion.2), kind=kOutput, calls=%fused_computation.98 | convolution fusion | flops 134479872 | bytes 4464768 | tf_op jit(solution)/shard_map/dot_general | solution.py:64
  15.3 0.3 fusion.66
  16.0 0.5 copy-done.11
  16.5 0.3 fusion.51
  16.8 0.6 multiply_bitcast_fusion
  17.5 0.3 convolution_convert_fusion.2
  17.7 0.8 pad_maximum_fusion.1
  18.5 0.7 broadcast_in_dim.19
  19.2 0.6 broadcast_in_dim.18
  19.8 36.4 %while.14 = (s32[]{:T(128)}, f32[32,1,8,2]{2,3,0,1:T(2,128)}, f32[32,1,8,2]{2,3,0,1:T(2,128)}, f32[32,1,8,2,128]{4,2,3,0,1:T(8,128)}, s32[]{:T(128)}, /*index=5*...) while((s32[]{:T(128)}, f32[32,1,8,2]{2,3,0,1:T(2,128)}, ...), condition=%wide.region_5.6_spmd, body=%wide.region_2.5_spmd.sunk | while | flops 51390212 | bytes 16918980 | solution.py:118
  19.8 3.2 %constant_dynamic-slice_fusion.2 = bf16[32,256,128]{2,1,0:T(8,128)(2,1)} fusion(bf16[32,1024,128]{2,1,0:T(8,128)(2,1)} %get-tuple-element.224, s32[]{:T(128)S(6)} %select_n.25), kind=kLoop, calls=%fused_computation.22.clone.1 | loop fusion | bytes 4194308 | tf_op jit(solution)/shard_map/while/body/dynamic_slice | solution.py:94
  23.0 3.3 %copy.81 = bf16[32,256,128]{1,2,0:T(8,128)(2,1)S(1)} copy(bf16[32,256,128]{2,1,0:T(8,128)(2,1)} %constant_dynamic-slice_fusion.2) | data formatting | bytes 4194304 | tf_op jit(solution)/shard_map/while/body/dynamic_slice | solution.py:94
  26.3 0.8 broadcast_compare_fusion.2
  27.1 1.4 fusion.98
  28.5 2.1 fusion.101
  30.6 0.3 fusion.100
  31.0 0.3 copy-done.8
  31.3 0.6 copy.91
  32.0 3.2 %constant_dynamic-slice_fusion.2 = bf16[32,256,128]{2,1,0:T(8,128)(2,1)} fusion(bf16[32,1024,128]{2,1,0:T(8,128)(2,1)} %get-tuple-element.224, s32[]{:T(128)S(6)} %select_n.25), kind=kLoop, calls=%fused_computation.22.clone.1 | loop fusion | bytes 4194308 | tf_op jit(solution)/shard_map/while/body/dynamic_slice | solution.py:94
  35.1 3.3 %copy.81 = bf16[32,256,128]{1,2,0:T(8,128)(2,1)S(1)} copy(bf16[32,256,128]{2,1,0:T(8,128)(2,1)} %constant_dynamic-slice_fusion.2) | data formatting | bytes 4194304 | tf_op jit(solution)/shard_map/while/body/dynamic_slice | solution.py:94
  38.4 0.8 broadcast_compare_fusion.2
  39.2 1.4 fusion.98
  40.7 2.1 fusion.101
  42.8 0.3 fusion.100
  43.1 0.3 copy-done.8
  43.5 0.6 copy.91
  44.1 3.2 %constant_dynamic-slice_fusion.2 = bf16[32,256,128]{2,1,0:T(8,128)(2,1)} fusion(bf16[32,1024,128]{2,1,0:T(8,128)(2,1)} %get-tuple-element.224, s32[]{:T(128)S(6)} %select_n.25), kind=kLoop, calls=%fused_computation.22.clone.1 | loop fusion | bytes 4194308 | tf_op jit(solution)/shard_map/while/body/dynamic_slice | solution.py:94
  47.3 3.3 %copy.81 = bf16[32,256,128]{1,2,0:T(8,128)(2,1)S(1)} copy(bf16[32,256,128]{2,1,0:T(8,128)(2,1)} %constant_dynamic-slice_fusion.2) | data formatting | bytes 4194304 | tf_op jit(solution)/shard_map/while/body/dynamic_slice | solution.py:94
  50.6 0.8 broadcast_compare_fusion.2
  51.3 1.4 fusion.98
  52.8 2.1 fusion.101
  54.9 0.3 fusion.100
  55.2 0.3 copy-done.8
  55.6 0.6 copy.91
  56.2 1.1 broadcast_divide_fusion
  57.3 0.8 fusion.50
  58.2 0.7 broadcast_bitcast_fusion
  59.1 3.7 %convolution_convert_fusion.1 = bf16[32,2048]{1,0:T(8,128)(2,1)} fusion(bf16[1024,2048]{1,0:T(8,128)(2,1)} %param.33, f32[4,8,8,128]{3,2,1,0:T(8,128)S(1)} %bitcast.178, f32[4,8,8,128]{3,2,1,0:T(8,128)S(1)} %bitcast.180, f32[4,8,8,128]{3,2,1,0:T(8,128)S(1)} %bitcast.179, f32[1024]{0:T(1024)S(1)} %get-tuple-element.126, f32[1024]{0:T(1024)S(1)} %get-tuple-element.127), kind=kOutput, calls=%fused_computation.24 | convolution fusion | flops 134447104 | bytes 4726784 | tf_op jit(solution)/shard_map/dot_general | solution.py:123
  62.9 32.9 %all-reduce.3.cloned.1.call-done = bf16[32,2048]{1,0:T(8,128)(2,1)} async-done(((bf16[32,2048]{1,0:T(8,128)(2,1)}), bf16[32,2048]{1,0:T(8,128)(2,1)}) %all-reduce.3.cloned.1.call-update) | async-done | bytes 131088 | tf_op jit(solution)/shard_map/psum | solution.py:122
  95.8 1.1 convert_add_fusion
  96.9 1.6 multiply_convert_fusion
  99.0 0.6 dynamic-slice
  100.4 1.1 broadcast_in_dim.20
  101.6 1.1 fusion.42
  102.9 42.2 %all-reduce = bf16[512]{0:T(512)(128)(2,1)S(1)} all-reduce(bf16[512]{0:T(512)(128)(2,1)S(1)} %dynamic-update-slice), channel_id=1, replica_groups=mesh['ep'=16,'tp'=2] {'ep'}, use_global_device_ids=true, to_apply=%add | all-reduce | flops 512 | bytes 2048
  145.1 15.5 %all-gather.2.cloned.1.call-done = bf16[512,2048]{1,0:T(8,128)(2,1)} async-done(((bf16[32,2048]{1,0:T(8,128)(2,1)}), bf16[512,2048]{1,0:T(8,128)(2,1)}) %all-gather.2.cloned.1.call-update) | async-done | bytes 2097168 | tf_op jit(solution)/shard_map/all_gather | solution.py:168
  160.6 2.6 fusion.68
  163.2 0.9 fusion.35
  164.1 2.1 all_gather.14
  166.2 2.1 convolution_multiply_fusion.1
  168.3 0.3 convolution_convert_fusion
  168.7 38.9 %all_to_all.10 = bf16[16,16,2048]{2,1,0:T(8,128)(2,1)S(1)} all-to-all(bf16[16,16,2048]{2,1,0:T(8,128)(2,1)S(1)} %bitcast.170), channel_id=1, replica_groups=mesh['ep'=16,'tp'=2] {'ep'}, dimensions={0} | all-to-all | bytes 2097152 | tf_op jit(solution)/shard_map/all_to_all | solution.py:145
  207.6 0.6 fusion.24
  208.2 0.6 fusion.32
  208.8 2.1 all_gather.12
  211.0 1.4 fusion.26
  212.4 4.3 %all-to-all-start.1 = ((bf16[16,16,1024]{2,1,0:T(8,128)(2,1)}), bf16[16,16,1024]{2,1,0:T(8,128)(2,1)S(1)}, u32[]{:S(2)}, u32[]{:S(2)}) async-start(bf16[16,16,1024]{2,1,0:T(8,128)(2,1)} %fusion.26), calls=%async_computation.1 | async-start | bytes 1048576 | tf_op jit(solution)/shard_map/all_to_all | solution.py:155
  217.0 0.7 convert_element_type.103
  217.8 18.3 %all-to-all-done.1 = bf16[16,16,1024]{2,1,0:T(8,128)(2,1)S(1)} async-done(((bf16[16,16,1024]{2,1,0:T(8,128)(2,1)}), bf16[16,16,1024]{2,1,0:T(8,128)(2,1)S(1)}, u32[]{:S(2)}, u32[]{:S(2)}) %all-to-all-start.1) | async-done | bytes 524320 | tf_op jit(solution)/shard_map/all_to_all | solution.py:155
  236.2 18.2 %reduce-scatter.2.cloned.1.call-done = f32[32,1024]{1,0:T(8,128)} async-done(((f32[512,1024]{1,0:T(8,128)}), f32[32,1024]{1,0:T(8,128)}) %reduce-scatter.2.cloned.1.call-update) | async-done | bytes 131088 | tf_op jit(solution)/shard_map/reduce_scatter | solution.py:176
  254.4 1.9 fusion.37
  (110 shorter events, 3.1 us)
Async XLA Ops:
  7.2 203.8 %copy-start = (bf16[1,704,1024]{2,1,0:T(8,128)(2,1)S(1)}, bf16[1,704,1024]{2,1,0:T(8,128)(2,1)}, u32[]{:S(2)}) copy-start(bf16[1,704,1024]{2,1,0:T(8,128)(2,1)} %param.39) | copy-start | bytes 4325380
  7.2 88.6 %all-reduce.3.cloned.1.call-start = ((), (), s32[]{:S(2)}) async-start(), calls=%async_computation.3 | async-start | bytes 262144 | tf_op jit(solution)/shard_map/psum | solution.py:122
  15.0 2.4 copy-start.1
  15.0 2.4 copy-start.10
  15.0 2.4 copy-start.13
  15.9 0.6 copy-start.11
  17.7 2.1 copy-start.14
  26.3 2.2 copy-start.3
  26.3 2.2 copy-start.7
  28.5 2.4 copy-start.4
  30.6 0.7 copy-start.8
  31.3 0.6 copy-start.5
  38.4 2.2 copy-start.3
  38.4 2.2 copy-start.7
  40.7 2.4 copy-start.4
  42.8 0.7 copy-start.8
  43.5 0.6 copy-start.5
  50.5 2.2 copy-start.3
  50.5 2.2 copy-start.7
  52.8 2.4 copy-start.4
  54.9 0.7 copy-start.8
  55.6 0.6 copy-start.5
  59.0 36.7 %copy-start.2 = (bf16[32,2048]{1,0:T(8,128)(2,1)S(1)}, bf16[32,2048]{1,0:T(8,128)(2,1)}, u32[]{:S(2)}) copy-start(bf16[32,2048]{1,0:T(8,128)(2,1)} %param.23) | copy-start | bytes 393220
  59.1 37.8 %copy-start.15 = (f32[2048]{0:T(1024)S(1)}, f32[2048]{0:T(1024)}, u32[]{:S(2)}) copy-start(f32[2048]{0:T(1024)} %param.34) | copy-start | bytes 24580
  59.1 39.5 %copy-start.17 = (s32[32,2]{0,1:T(2,128)S(1)}, s32[32,2]{0,1:T(2,128)}, u32[]{:S(2)}) copy-start(s32[32,2]{0,1:T(2,128)} %param.35) | copy-start | bytes 772
  59.1 39.9 %copy-start.16 = (bf16[2048]{0:T(1024)(128)(2,1)S(1)}, bf16[2048]{0:T(1024)(128)(2,1)}, u32[]{:S(2)}) copy-start(bf16[2048]{0:T(1024)(128)(2,1)} %param.40) | copy-start | bytes 12292
  59.1 39.9 %copy-start.23 = (u32[32]{0:T(128)S(1)}, u32[32]{0:T(128)}, u32[]{:S(2)}) copy-start(u32[32]{0:T(128)} %constant.84) | copy-start | bytes 388
  62.8 97.8 %copy-start.21 = (bf16[2048,176]{0,1:T(8,128)(2,1)S(1)}, bf16[2048,176]{0,1:T(8,128)(2,1)}, u32[]{:S(2)}) copy-start(bf16[2048,176]{0,1:T(8,128)(2,1)} %param.41) | copy-start | bytes 2162692
  62.9 97.7 %all-gather.2.cloned.1.call-start = ((), (), s32[]{:S(2)}) async-start(), calls=%async_computation.4 | async-start | bytes 2228224 | tf_op jit(solution)/shard_map/all_gather | solution.py:168
  98.5 155.9 %reduce-scatter.2.cloned.1.call-start = ((), (), s32[]{:S(2)}) async-start(), calls=%async_computation.5 | async-start | bytes 2228224 | tf_op jit(solution)/shard_map/reduce_scatter | solution.py:176
  160.6 2.6 copy-start.19
  160.6 2.6 copy-start.22
  163.2 2.9 %copy-start.9 = (bf16[352,1024]{1,0:T(8,128)(2,1)S(1)}, bf16[352,1024]{1,0:T(8,128)(2,1)}, u32[]{:S(2)}) copy-start(bf16[352,1024]{1,0:T(8,128)(2,1)} %param.43) | copy-start | bytes 2162692
  168.3 39.3 %copy-start.6 = (bf16[1,2048,352]{1,2,0:T(8,128)(2,1)S(1)}, bf16[1,2048,352]{1,2,0:T(8,128)(2,1)}, u32[]{:S(2)}) copy-start(bf16[1,2048,352]{1,2,0:T(8,128)(2,1)} %param.37) | copy-start | bytes 4325380
  168.7 39.5 %copy-start.20 = (bf16[1,2048,352]{1,2,0:T(8,128)(2,1)S(1)}, bf16[1,2048,352]{1,2,0:T(8,128)(2,1)}, u32[]{:S(2)}) copy-start(bf16[1,2048,352]{1,2,0:T(8,128)(2,1)} %param.38) | copy-start | bytes 4325380
  210.8 6.1 %copy-start.12 = (bf16[32,1,2,32]{3,2,0,1:T(2,128)(2,1)S(1)}, bf16[32,1,2,32]{3,2,0,1:T(2,128)(2,1)}, u32[]{:S(2)}) copy-start(bf16[32,1,2,32]{3,2,0,1:T(2,128)(2,1)} %copy-done.11) | copy-start | bytes 12292
  210.8 6.9 %copy-start.18 = (f32[32,2]{0,1:T(2,128)S(1)}, f32[32,2]{0,1:T(2,128)}, u32[]{:S(2)}) copy-start(f32[32,2]{0,1:T(2,128)} %param.36) | copy-start | bytes 772
  212.4 23.7 %all-to-all-start.1 = ((bf16[16,16,1024]{2,1,0:T(8,128)(2,1)}), bf16[16,16,1024]{2,1,0:T(8,128)(2,1)S(1)}, u32[]{:S(2)}, u32[]{:S(2)}) async-start(bf16[16,16,1024]{2,1,0:T(8,128)(2,1)} %fusion.26), calls=%async_computation.1 | async-start | bytes 1048576 | tf_op jit(solution)/shard_map/all_to_all | solution.py:155
Sparse Core Ops, SparseCore 0:
  63.0 32.7 all-reduce.2
  98.6 61.9 all-gather.1
  168.4 85.9 reduce-scatter.1
where the time goes:
time: 264 us; the launch traced here: 263 us
  blocking collectives  85.2 us (32%)
  waiting for transfers between devices  84.9 us (32%)
  matrix products  30.5 us (12%)
  local copies, waits for them, and re-layouts  29 us (11%)
  between operations  15.5 us (6%)
  other arithmetic  13 us (5%)
  starting transfers between devices  4.45 us (2%)
    unnamed x1, blocking collectives  42.2 us
    all_to_all x1, blocking collectives, per_device(): lax.all_to_all(outgoing, 'ep', split_axis=0, concat_axis=0, tiled=True)  38.9 us
    psum x1, waiting for transfers between devices, per_device(): lax.psum(jnp.dot(head_out, w_out, preferred_element_type=jnp.float32).ast...  32.9 us
    dynamic_slice x6, local copies, waits for them, and re-layouts, visit(): lax.dynamic_slice_in_dim(key_cache, offset, span_len, 1)  19.3 us
    all_to_all x1, waiting for transfers between devices, per_device(): lax.all_to_all(partial_value.astype(jnp.bfloat16), 'ep', split_axis=0, co...  18.3 us
    reduce_scatter x1, waiting for transfers between devices, per_device(): lax.psum_scatter(jnp.dot(dense_act, dense_down, preferred_element_type=jn...  18.2 us
    all_gather x1, waiting for transfers between devices, per_device(): lax.all_gather(moe_in, 'ep', axis=0, tiled=True)  15.5 us
    dot_general x3, matrix products, visit(): jnp.einsum('sgaml,slge->sgame', weights.astype(jnp.bfloat16), cached, pre...  6.25 us
  transfers between devices with their start and end apart: 4, of which 4 were waited for; matrix products, arithmetic and copies ran while one was open for 3% of the time, Pallas kernels for 0%

commit v1 on v0

--- a/solution.py
+++ b/solution.py
@@ -119,8 +119,11 @@
     mapped = summed / totals[..., None]
     head_mix = mapped[..., 0, :] - lambdas.reshape(1, kv_here, per_key, 1) * mapped[..., 1, :]
     head_out = rms_rows(head_mix, head_gain).astype(jnp.bfloat16).reshape(batch_rows, -1)
-    attn_out = lax.psum(
-        jnp.dot(head_out, w_out, preferred_element_type=jnp.float32).astype(jnp.bfloat16), "tp"
+    attn_out = jnp.sum(
+        lax.all_gather(
+            jnp.dot(head_out, w_out, preferred_element_type=jnp.float32).astype(jnp.bfloat16), "tp"
+        ),
+        axis=0,
     )
     residual = hidden_in.astype(jnp.float32) + attn_out.astype(jnp.float32)
     moe_in = rms_rows(residual, ffn_gain).astype(jnp.bfloat16)

time: 264 us -> 245 us (0.928)
  waiting for transfers between devices: 84.9 us -> 52.8 us
  blocking collectives: 85.2 us -> 101 us
    psum x1 -> x0, waiting for transfers between devices: 32.9 us -> none  [per_device(): lax.psum(jnp.dot(head_out, w_out, preferred_element_type=jnp.float32).ast...]
    unnamed x1, blocking collectives: 42.2 us -> 55.7 us
  transfers between devices with their start and end apart: 4 -> 3, of which waited for: 4 -> 3; matrix products, arithmetic and copies ran while one was open for 3% -> 3% of each run, Pallas kernels for 0% -> 0%
where the time goes in v1:
time: 245 us; the launch traced here: 244 us
  blocking collectives  101 us (41%)
  waiting for transfers between devices  52.8 us (22%)
  matrix products  29.8 us (12%)
  local copies, waits for them, and re-layouts  29 us (12%)
  between operations  15.8 us (6%)
  other arithmetic  11.3 us (5%)
  starting transfers between devices  4.45 us (2%)
    unnamed x1, blocking collectives  55.7 us
    all_to_all x1, blocking collectives, per_device(): lax.all_to_all(outgoing, 'ep', split_axis=0, concat_axis=0, tiled=True)  38.9 us
    dynamic_slice x6, local copies, waits for them, and re-layouts, visit(): lax.dynamic_slice_in_dim(key_cache, offset, span_len, 1)  19.2 us
    reduce_scatter x1, waiting for transfers between devices, per_device(): lax.psum_scatter(jnp.dot(dense_act, dense_down, preferred_element_type=jn...  19.2 us
    all_to_all x1, waiting for transfers between devices, per_device(): lax.all_to_all(partial_value.astype(jnp.bfloat16), 'ep', split_axis=0, co...  18.1 us
    all_gather x1, waiting for transfers between devices, per_device(): lax.all_gather(moe_in, 'ep', axis=0, tiled=True)  15.5 us
    dot_general x3, matrix products, visit(): jnp.einsum('sgaml,slge->sgame', weights.astype(jnp.bfloat16), cached, pre...  6.24 us
  transfers between devices with their start and end apart: 3, of which 3 were waited for; matrix products, arithmetic and copies ran while one was open for 3% of the time, Pallas kernels for 0%

profile of v1, /device:TPU:0, one launch (start us, length us, event | category | flops | bytes accessed | tf_op | source)
XLA Modules:
  0.0 244.4 jit_solution(9492527208004837848)
XLA Ops:
  7.2 1.4 fusion.67
  9.3 1.0 fusion.43
  10.4 1.4 fusion.62
  11.9 3.2 %fusion.60 = f32[32,1024]{1,0:T(8,128)S(1)} fusion(bf16[2048,1024]{1,0:T(8,128)(2,1)} %param.28, bf16[32,2048]{1,0:T(8,128)(2,1)} %param.23, f32[2048]{0:T(1024)} %param.27, f32[32]{0:T(128)S(1)} %add_rsqrt_fusion.2), kind=kOutput, calls=%fused_computation.98 | convolution fusion | flops 134479872 | bytes 4464768 | tf_op jit(solution)/shard_map/dot_general | solution.py:64
  15.3 0.3 fusion.66
  16.0 0.5 copy-done.11
  16.5 0.3 fusion.51
  16.8 0.6 multiply_bitcast_fusion
  17.5 0.3 convolution_convert_fusion.2
  17.7 0.8 pad_maximum_fusion.1
  18.5 0.7 broadcast_in_dim.19
  19.2 0.6 broadcast_in_dim.18
  19.9 36.4 %while.14 = (s32[]{:T(128)}, f32[32,1,8,2]{2,3,0,1:T(2,128)}, f32[32,1,8,2]{2,3,0,1:T(2,128)}, f32[32,1,8,2,128]{4,2,3,0,1:T(8,128)}, s32[]{:T(128)}, /*index=5*...) while((s32[]{:T(128)}, f32[32,1,8,2]{2,3,0,1:T(2,128)}, ...), condition=%wide.region_5.6_spmd, body=%wide.region_2.5_spmd.sunk | while | flops 51390212 | bytes 16918980 | solution.py:118
  19.9 3.1 %constant_dynamic-slice_fusion.2 = bf16[32,256,128]{2,1,0:T(8,128)(2,1)} fusion(bf16[32,1024,128]{2,1,0:T(8,128)(2,1)} %get-tuple-element.224, s32[]{:T(128)S(6)} %select_n.25), kind=kLoop, calls=%fused_computation.22.clone.1 | loop fusion | bytes 4194308 | tf_op jit(solution)/shard_map/while/body/dynamic_slice | solution.py:94
  23.0 3.3 %copy.81 = bf16[32,256,128]{1,2,0:T(8,128)(2,1)S(1)} copy(bf16[32,256,128]{2,1,0:T(8,128)(2,1)} %constant_dynamic-slice_fusion.2) | data formatting | bytes 4194304 | tf_op jit(solution)/shard_map/while/body/dynamic_slice | solution.py:94
  26.3 0.8 broadcast_compare_fusion.2
  27.1 1.4 fusion.98
  28.5 2.1 fusion.101
  30.6 0.3 fusion.100
  31.0 0.4 copy-done.8
  31.3 0.6 copy.91
  32.0 3.1 %constant_dynamic-slice_fusion.2 = bf16[32,256,128]{2,1,0:T(8,128)(2,1)} fusion(bf16[32,1024,128]{2,1,0:T(8,128)(2,1)} %get-tuple-element.224, s32[]{:T(128)S(6)} %select_n.25), kind=kLoop, calls=%fused_computation.22.clone.1 | loop fusion | bytes 4194308 | tf_op jit(solution)/shard_map/while/body/dynamic_slice | solution.py:94
  35.1 3.3 %copy.81 = bf16[32,256,128]{1,2,0:T(8,128)(2,1)S(1)} copy(bf16[32,256,128]{2,1,0:T(8,128)(2,1)} %constant_dynamic-slice_fusion.2) | data formatting | bytes 4194304 | tf_op jit(solution)/shard_map/while/body/dynamic_slice | solution.py:94
  38.4 0.8 broadcast_compare_fusion.2
  39.2 1.4 fusion.98
  40.7 2.1 fusion.101
  42.8 0.3 fusion.100
  43.1 0.4 copy-done.8
  43.5 0.6 copy.91
  44.1 3.1 %constant_dynamic-slice_fusion.2 = bf16[32,256,128]{2,1,0:T(8,128)(2,1)} fusion(bf16[32,1024,128]{2,1,0:T(8,128)(2,1)} %get-tuple-element.224, s32[]{:T(128)S(6)} %select_n.25), kind=kLoop, calls=%fused_computation.22.clone.1 | loop fusion | bytes 4194308 | tf_op jit(solution)/shard_map/while/body/dynamic_slice | solution.py:94
  47.2 3.3 %copy.81 = bf16[32,256,128]{1,2,0:T(8,128)(2,1)S(1)} copy(bf16[32,256,128]{2,1,0:T(8,128)(2,1)} %constant_dynamic-slice_fusion.2) | data formatting | bytes 4194304 | tf_op jit(solution)/shard_map/while/body/dynamic_slice | solution.py:94
  50.5 0.8 broadcast_compare_fusion.2
  51.3 1.4 fusion.98
  52.8 2.1 fusion.101
  54.9 0.3 fusion.100
  55.2 0.4 copy-done.8
  55.6 0.6 copy.91
  56.2 1.1 broadcast_divide_fusion
  57.3 0.8 fusion.50
  58.2 0.7 broadcast_bitcast_fusion
  59.1 3.0 %convolution_convert_fusion.1 = bf16[32,2048]{1,0:T(8,128)(2,1)S(1)} fusion(bf16[1024,2048]{1,0:T(8,128)(2,1)} %param.33, f32[4,8,8,128]{3,2,1,0:T(8,128)S(1)} %bitcast.180, f32[4,8,8,128]{3,2,1,0:T(8,128)S(1)} %bitcast.182, f32[4,8,8,128]{3,2,1,0:T(8,128)S(1)} %bitcast.181, f32[1024]{0:T(1024)S(1)} %get-tuple-element.126, f32[1024]{0:T(1024)S(1)} %get-tuple-element.127), kind=kOutput, calls=%fused_computation.24 | convolution fusion | flops 134447104 | bytes 4726784 | tf_op jit(solution)/shard_map/dot_general | solution.py:124
  62.1 2.3 all-gather
  64.6 0.7 multiply_convert_fusion
  65.5 1.1 broadcast_in_dim.20
  67.0 0.6 dynamic-slice
  68.3 1.1 fusion.42
  69.3 0.2 dynamic-update-slice
  69.6 55.7 %all-reduce = bf16[512]{0:T(512)(128)(2,1)S(1)} all-reduce(bf16[512]{0:T(512)(128)(2,1)S(1)} %dynamic-update-slice), channel_id=1, replica_groups=mesh['ep'=16,'tp'=2] {'ep'}, use_global_device_ids=true, to_apply=%add | all-reduce | flops 512 | bytes 2048
  125.5 15.5 %all-gather.3.cloned.1.call-done = bf16[512,2048]{1,0:T(8,128)(2,1)} async-done(((bf16[32,2048]{1,0:T(8,128)(2,1)}), bf16[512,2048]{1,0:T(8,128)(2,1)}) %all-gather.3.cloned.1.call-update) | async-done | bytes 2097168 | tf_op jit(solution)/shard_map/all_gather | solution.py:171
  141.0 2.6 %fusion.68 = f32[512,176]{0,1:T(8,128)S(1)} fusion(bf16[512,2048]{1,0:T(8,128)(2,1)} %all-gather.3.cloned.1.call-done, bf16[2048,176]{0,1:T(8,128)(2,1)S(1)} %copy-done.21), kind=kOutput, calls=%fused_computation.104 | convolution fusion | flops 369098752 | bytes 3178496 | tf_op jit(solution)/shard_map/dot_general | solution.py:174
  143.6 0.9 fusion.35
  144.5 2.1 all_gather.22
  146.5 2.1 convolution_multiply_fusion.1
  148.6 0.3 convolution_convert_fusion
  149.1 38.9 %all_to_all.10 = bf16[16,16,2048]{2,1,0:T(8,128)(2,1)S(1)} all-to-all(bf16[16,16,2048]{2,1,0:T(8,128)(2,1)S(1)} %bitcast.171), channel_id=1, replica_groups=mesh['ep'=16,'tp'=2] {'ep'}, dimensions={0} | all-to-all | bytes 2097152 | tf_op jit(solution)/shard_map/all_to_all | solution.py:148
  187.9 0.6 fusion.24
  188.5 0.6 fusion.32
  189.1 2.1 all_gather.20
  191.4 1.4 fusion.26
  192.7 4.4 %all-to-all-start.1 = ((bf16[16,16,1024]{2,1,0:T(8,128)(2,1)}), bf16[16,16,1024]{2,1,0:T(8,128)(2,1)S(1)}, u32[]{:S(2)}, u32[]{:S(2)}) async-start(bf16[16,16,1024]{2,1,0:T(8,128)(2,1)} %fusion.26), calls=%async_computation.1 | async-start | bytes 1048576 | tf_op jit(solution)/shard_map/all_to_all | solution.py:158
  197.4 0.7 convert_element_type.105
  198.2 18.1 %all-to-all-done.1 = bf16[16,16,1024]{2,1,0:T(8,128)(2,1)S(1)} async-done(((bf16[16,16,1024]{2,1,0:T(8,128)(2,1)}), bf16[16,16,1024]{2,1,0:T(8,128)(2,1)S(1)}, u32[]{:S(2)}, u32[]{:S(2)}) %all-to-all-start.1) | async-done | bytes 524320 | tf_op jit(solution)/shard_map/all_to_all | solution.py:158
  216.4 19.2 %reduce-scatter.2.cloned.1.call-done = f32[32,1024]{1,0:T(8,128)} async-done(((f32[512,1024]{1,0:T(8,128)}), f32[32,1024]{1,0:T(8,128)}) %reduce-scatter.2.cloned.1.call-update) | async-done | bytes 131088 | tf_op jit(solution)/shard_map/reduce_scatter | solution.py:179
  235.6 1.9 fusion.37
  (109 shorter events, 3.0 us)
Async XLA Ops:
  7.2 184.2 %copy-start = (bf16[1,704,1024]{2,1,0:T(8,128)(2,1)S(1)}, bf16[1,704,1024]{2,1,0:T(8,128)(2,1)}, u32[]{:S(2)}) copy-start(bf16[1,704,1024]{2,1,0:T(8,128)(2,1)} %param.39) | copy-start | bytes 4325380
  7.2 133.8 %all-gather.3.cloned.1.call-start = ((), (), s32[]{:S(2)}) async-start(), calls=%async_computation.3 | async-start | bytes 2228224 | tf_op jit(solution)/shard_map/all_gather | solution.py:171
  15.0 2.4 copy-start.1
  15.0 2.4 copy-start.10
  15.0 2.4 copy-start.13
  15.9 0.6 copy-start.11
  17.7 2.1 copy-start.14
  26.3 2.2 copy-start.3
  26.3 2.2 copy-start.7
  28.5 2.4 copy-start.4
  30.6 0.7 copy-start.8
  31.3 0.6 copy-start.5
  38.4 2.2 copy-start.3
  38.4 2.2 copy-start.7
  40.7 2.4 copy-start.4
  42.7 0.7 copy-start.8
  43.5 0.6 copy-start.5
  50.5 2.2 copy-start.3
  50.5 2.2 copy-start.7
  52.8 2.4 copy-start.4
  54.9 0.7 copy-start.8
  55.6 0.6 copy-start.5
  59.0 5.4 %copy-start.2 = (bf16[32,2048]{1,0:T(8,128)(2,1)S(1)}, bf16[32,2048]{1,0:T(8,128)(2,1)}, u32[]{:S(2)}) copy-start(bf16[32,2048]{1,0:T(8,128)(2,1)} %param.23) | copy-start | bytes 393220
  59.1 5.6 %copy-start.15 = (f32[2048]{0:T(1024)S(1)}, f32[2048]{0:T(1024)}, u32[]{:S(2)}) copy-start(f32[2048]{0:T(1024)} %param.34) | copy-start | bytes 24580
  62.1 4.5 %copy-start.17 = (s32[32,2]{0,1:T(2,128)S(1)}, s32[32,2]{0,1:T(2,128)}, u32[]{:S(2)}) copy-start(s32[32,2]{0,1:T(2,128)} %param.35) | copy-start | bytes 772
  62.1 4.9 %copy-start.16 = (bf16[2048]{0:T(1024)(128)(2,1)S(1)}, bf16[2048]{0:T(1024)(128)(2,1)}, u32[]{:S(2)}) copy-start(bf16[2048]{0:T(1024)(128)(2,1)} %param.40) | copy-start | bytes 12292
  62.1 4.9 %copy-start.23 = (u32[32]{0:T(128)S(1)}, u32[32]{0:T(128)}, u32[]{:S(2)}) copy-start(u32[32]{0:T(128)} %constant.86) | copy-start | bytes 388
  62.1 78.8 %copy-start.21 = (bf16[2048,176]{0,1:T(8,128)(2,1)S(1)}, bf16[2048,176]{0,1:T(8,128)(2,1)}, u32[]{:S(2)}) copy-start(bf16[2048,176]{0,1:T(8,128)(2,1)} %param.41) | copy-start | bytes 2162692
  65.4 170.2 %reduce-scatter.2.cloned.1.call-start = ((), (), s32[]{:S(2)}) async-start(), calls=%async_computation.4 | async-start | bytes 2228224 | tf_op jit(solution)/shard_map/reduce_scatter | solution.py:179
  141.0 2.6 %copy-start.19 = (bf16[512,2048]{1,0:T(8,128)(2,1)S(1)}, bf16[512,2048]{1,0:T(8,128)(2,1)}, u32[]{:S(2)}) copy-start(bf16[512,2048]{1,0:T(8,128)(2,1)} %all-gather.3.cloned.1.call-done) | copy-start | bytes 6291460
  141.0 2.6 %copy-start.22 = (bf16[2048,176]{0,1:T(8,128)(2,1)S(1)}, bf16[2048,176]{0,1:T(8,128)(2,1)}, u32[]{:S(2)}) copy-start(bf16[2048,176]{0,1:T(8,128)(2,1)} %param.42) | copy-start | bytes 2162692
  143.6 2.9 %copy-start.9 = (bf16[352,1024]{1,0:T(8,128)(2,1)S(1)}, bf16[352,1024]{1,0:T(8,128)(2,1)}, u32[]{:S(2)}) copy-start(bf16[352,1024]{1,0:T(8,128)(2,1)} %param.43) | copy-start | bytes 2162692
  148.6 39.3 %copy-start.6 = (bf16[1,2048,352]{1,2,0:T(8,128)(2,1)S(1)}, bf16[1,2048,352]{1,2,0:T(8,128)(2,1)}, u32[]{:S(2)}) copy-start(bf16[1,2048,352]{1,2,0:T(8,128)(2,1)} %param.37) | copy-start | bytes 4325380
  149.0 39.5 %copy-start.20 = (bf16[1,2048,352]{1,2,0:T(8,128)(2,1)S(1)}, bf16[1,2048,352]{1,2,0:T(8,128)(2,1)}, u32[]{:S(2)}) copy-start(bf16[1,2048,352]{1,2,0:T(8,128)(2,1)} %param.38) | copy-start | bytes 4325380
  191.2 6.1 %copy-start.12 = (bf16[32,1,2,32]{3,2,0,1:T(2,128)(2,1)S(1)}, bf16[32,1,2,32]{3,2,0,1:T(2,128)(2,1)}, u32[]{:S(2)}) copy-start(bf16[32,1,2,32]{3,2,0,1:T(2,128)(2,1)} %copy-done.11) | copy-start | bytes 12292
  191.2 6.9 %copy-start.18 = (f32[32,2]{0,1:T(2,128)S(1)}, f32[32,2]{0,1:T(2,128)}, u32[]{:S(2)}) copy-start(f32[32,2]{0,1:T(2,128)} %param.36) | copy-start | bytes 772
  192.7 23.6 %all-to-all-start.1 = ((bf16[16,16,1024]{2,1,0:T(8,128)(2,1)}), bf16[16,16,1024]{2,1,0:T(8,128)(2,1)S(1)}, u32[]{:S(2)}, u32[]{:S(2)}) async-start(bf16[16,16,1024]{2,1,0:T(8,128)(2,1)} %fusion.26), calls=%async_computation.1 | async-start | bytes 1048576 | tf_op jit(solution)/shard_map/all_to_all | solution.py:158
Sparse Core Ops, SparseCore 0:
  65.5 75.4 all-gather.2
  148.7 86.8 reduce-scatter.1
